TPU v7x, 32 devices: a whole 2x2x4 slice. The times are simulated.
32 devices in a mesh: ep: 4 (over y, x), tp: 8 (over z, core).
Axes of the slice: x: 2, y: 2, z: 4, core: 2. Of those that a mesh axis runs over, the one named last changes fastest.
Arguments:
- tokens: bfloat16 [256, 4096], P('ep'), may hold values from -6 to 6
- norm_gain: float32 [4096], replicated, may hold values from 0.1 to 1.9
- ffn_gain: float32 [4096], replicated, may hold values from 0.1 to 1.9
- w_in: bfloat16 [4096, 2048], P(None, 'tp'), may hold values from -0.09375 to 0.09375
- decay_rate: float32 [8192], P('tp'), may hold values from 0.02 to 2
- frequency: float32 [8192], P('tp'), may hold values from -3.140625 to 3.140625
- log_step: float32 [128], P('tp'), may hold values from -2.3 to 0
- input_real: float32 [16, 8192], P(None, 'tp'), may hold values from -1 to 1
- input_imag: float32 [16, 8192], P(None, 'tp'), may hold values from -1 to 1
- readout_real: float32 [16, 8192], P(None, 'tp'), may hold values from -0.5 to 0.5
- readout_imag: float32 [16, 8192], P(None, 'tp'), may hold values from -0.5 to 0.5
- skip_gain: float32 [2048], P('tp'), may hold values from -4 to 4
- state_real: float32 [256, 8192], P('ep', 'tp'), may hold values from -6 to 6
- state_imag: float32 [256, 8192], P('ep', 'tp'), may hold values from -6 to 6
- w_out: bfloat16 [2048, 4096], P('tp'), may hold values from -0.125 to 0.125
- shared_gate: bfloat16 [4096, 1024], P(None, 'tp'), may hold values from -0.09375 to 0.09375
- shared_up: bfloat16 [4096, 1024], P(None, 'tp'), may hold values from -0.09375 to 0.09375
- shared_down: bfloat16 [1024, 4096], P('tp'), may hold values from -0.1875 to 0.1875
- expert_gate: bfloat16 [16, 4096, 1024], P('ep', 'tp'), may hold values from -0.09375 to 0.09375
- expert_up: bfloat16 [16, 4096, 1024], P('ep', 'tp'), may hold values from -0.09375 to 0.09375
- expert_down: bfloat16 [16, 1024, 4096], P('ep', None, 'tp'), may hold values from -0.1875 to 0.1875
- routing: int32 [256, 4], P('ep'), may hold values from 0 to 15, all different within a row; in each aligned block of 64 rows (0 to 63, 64 to 127, ...) at most 32 rows name the same one
- route_weight: float32 [256, 4], P('ep'), may hold values from 0.1 to 1
Outputs:
- mixed: bfloat16 [256, 4096], P('ep', 'tp')
- new_state_real: float32 [256, 8192], P('ep', 'tp')
- new_state_imag: float32 [256, 8192], P('ep', 'tp')
Inputs may be any that keep to these rules, and one draw needn't show every extreme that they name: `routing`: each row names 4 different experts. In the rows of one index of ep (aligned blocks of 64 rows) no expert is named more than 32 times, and in every draw some expert is named exactly 32 times in some block.
All inputs are finite; a program needn't handle non-finite values.
Results may differ from a plain program's by a relative error of at most 0.02.
Values may be sent and summed in bfloat16 or wider, within the bound.
A program may use at most 64 MiB of HBM per device.

v0:
```python
import jax
import jax.numpy as jnp
from jax import lax
from jax.sharding import PartitionSpec as P

EPS = 1e-06
ROUTED_SCALE = 2.5
HIGH = lax.Precision.HIGHEST


def rms_scale(values_in, gains):
    values = values_in.astype(jnp.float32)
    factor = lax.rsqrt(jnp.mean(values * values, axis=-1, keepdims=True) + EPS)
    return (values * factor * gains).astype(jnp.bfloat16)


def state_update(
    normed,
    w_in,
    decay_rate,
    frequency,
    log_step,
    input_real,
    input_imag,
    readout_real,
    readout_imag,
    skip_gain,
    state_real,
    state_imag,
):
    seq_count = normed.shape[0]
    groups = log_step.shape[0]
    chan_count = skip_gain.shape[0] // groups
    state_width = decay_rate.shape[0] // groups
    drive_rows = jnp.dot(normed, w_in, preferred_element_type=jnp.float32).astype(jnp.bfloat16)
    drive_f = drive_rows.astype(jnp.float32).reshape(seq_count, groups, chan_count)
    decays = decay_rate.reshape(groups, state_width)
    omegas = frequency.reshape(groups, state_width)
    step_size = jnp.exp(log_step)[:, None]
    pole_mag = jnp.exp(-decays * step_size)
    pole_angle = omegas * step_size
    pole_re = pole_mag * jnp.cos(pole_angle)
    pole_im = pole_mag * jnp.sin(pole_angle)
    pole_norm = decays * decays + omegas * omegas
    diff_re = pole_re - 1.0
    lift_re = (-decays * diff_re + omegas * pole_im) / pole_norm
    lift_im = (-decays * pole_im - omegas * diff_re) / pole_norm
    in_re = input_real.reshape(chan_count, groups, state_width)
    in_im = input_imag.reshape(chan_count, groups, state_width)
    push_re = jnp.einsum("sgh,hgp->sgp", drive_f, in_re, precision=HIGH)
    push_im = jnp.einsum("sgh,hgp->sgp", drive_f, in_im, precision=HIGH)
    old_re = state_real.reshape(seq_count, groups, state_width)
    old_im = state_imag.reshape(seq_count, groups, state_width)
    new_re = pole_re * old_re - pole_im * old_im + lift_re * push_re - lift_im * push_im
    new_im = pole_re * old_im + pole_im * old_re + lift_re * push_im + lift_im * push_re
    out_re = readout_real.reshape(chan_count, groups, state_width)
    out_im = readout_imag.reshape(chan_count, groups, state_width)
    read_rows = jnp.einsum("sgp,hgp->sgh", new_re, out_re, precision=HIGH) - jnp.einsum(
        "sgp,hgp->sgh", new_im, out_im, precision=HIGH
    )
    read_rows = read_rows + skip_gain.reshape(groups, chan_count) * drive_f
    activated = jax.nn.gelu(read_rows).reshape(seq_count, groups * chan_count).astype(jnp.bfloat16)
    return (
        activated,
        new_re.reshape(seq_count, groups * state_width),
        new_im.reshape(seq_count, groups * state_width),
    )


def local(
    tokens,
    norm_gain,
    ffn_gain,
    w_in,
    decay_rate,
    frequency,
    log_step,
    input_real,
    input_imag,
    readout_real,
    readout_imag,
    skip_gain,
    state_real,
    state_imag,
    w_out,
    shared_gate,
    shared_up,
    shared_down,
    expert_gate,
    expert_up,
    expert_down,
    routing,
    route_weight,
):
    seq_count, model_width = tokens.shape
    tp_count = lax.axis_size("tp")
    ep_count = lax.axis_size("ep")
    slice_width = model_width // tp_count
    offset = lax.axis_index("tp") * slice_width
    normed = rms_scale(tokens, norm_gain)
    activated, new_real, new_imag = state_update(
        normed,
        w_in,
        decay_rate,
        frequency,
        log_step,
        input_real,
        input_imag,
        readout_real,
        readout_imag,
        skip_gain,
        state_real,
        state_imag,
    )
    mixer_terms = jnp.dot(activated, w_out, preferred_element_type=jnp.float32)
    mixer_own = lax.psum_scatter(mixer_terms, "tp", scatter_dimension=1, tiled=True)
    own_tokens = lax.dynamic_slice_in_dim(tokens, offset, slice_width, 1)
    resid_own = (own_tokens.astype(jnp.float32) + mixer_own).astype(jnp.bfloat16)
    resid_f = resid_own.astype(jnp.float32)
    square_sum = lax.psum(jnp.sum(resid_f * resid_f, axis=1, keepdims=True), "tp")
    factor = lax.rsqrt(square_sum / model_width + EPS)
    gain_own = lax.dynamic_slice_in_dim(ffn_gain, offset, slice_width, 0)
    rows_own = (resid_f * factor * gain_own).astype(jnp.bfloat16)
    ffn_rows = lax.all_gather(rows_own, "tp", axis=1, tiled=True)
    expert_dev = expert_gate.shape[0]
    expert_count = expert_dev * ep_count
    top_count = routing.shape[1]
    capacity = 2 * seq_count * top_count // expert_count
    slot_count = expert_count * capacity
    flat_ids = routing.reshape(-1)
    one_hot = (flat_ids[:, None] == jnp.arange(expert_count, dtype=jnp.int32)[None, :]).astype(
        jnp.int32
    )
    earlier = jnp.cumsum(one_hot, axis=0) - one_hot
    slot_rank = jnp.sum(earlier * one_hot, axis=1)
    target = flat_ids * capacity + slot_rank
    slot_ids = jnp.arange(slot_count, dtype=jnp.int32)
    placed = (target[None, :] == slot_ids[:, None]).reshape(slot_count, seq_count, top_count)
    dispatch_map = jnp.sum(placed.astype(jnp.float32), axis=2).astype(jnp.bfloat16)
    outgoing = jnp.dot(dispatch_map, rows_own, preferred_element_type=jnp.float32).astype(
        jnp.bfloat16
    )
    outgoing = outgoing.reshape(ep_count, expert_dev * capacity, slice_width)
    incoming = lax.all_to_all(outgoing, "ep", split_axis=0, concat_axis=0, tiled=True)
    arrived = incoming.reshape(ep_count, expert_dev, capacity, slice_width)
    gate_part = jnp.einsum(
        "secd,edf->secf", arrived, expert_gate, preferred_element_type=jnp.float32
    )
    up_part = jnp.einsum("secd,edf->secf", arrived, expert_up, preferred_element_type=jnp.float32)
    gate_full, up_full = (
        lax.psum(gate_part.astype(jnp.bfloat16), "tp").astype(jnp.float32),
        lax.psum(up_part.astype(jnp.bfloat16), "tp").astype(jnp.float32),
    )
    inner_rows = (jax.nn.silu(gate_full) * up_full).astype(jnp.bfloat16)
    expert_terms = jnp.einsum(
        "secf,efd->secd", inner_rows, expert_down, preferred_element_type=jnp.float32
    )
    returned = lax.all_to_all(
        expert_terms.reshape(ep_count, expert_dev * capacity, slice_width).astype(jnp.bfloat16),
        "ep",
        split_axis=0,
        concat_axis=0,
        tiled=True,
    ).astype(jnp.float32)
    weights = route_weight / jnp.sum(route_weight, axis=1, keepdims=True) * ROUTED_SCALE
    chosen = target.reshape(seq_count, top_count)[:, :, None] == slot_ids[None, None, :]
    combine = jnp.sum(jnp.where(chosen, weights[:, :, None], 0.0), axis=1)
    routed = jnp.dot(combine, returned.reshape(slot_count, slice_width), precision=HIGH)
    shared_gate_rows = jnp.dot(ffn_rows, shared_gate, preferred_element_type=jnp.float32)
    shared_up_rows = jnp.dot(ffn_rows, shared_up, preferred_element_type=jnp.float32)
    shared_inner = (jax.nn.silu(shared_gate_rows) * shared_up_rows).astype(jnp.bfloat16)
    shared_terms = jnp.dot(shared_inner, shared_down, preferred_element_type=jnp.float32)
    shared_own = lax.psum_scatter(
        shared_terms.astype(jnp.bfloat16), "tp", scatter_dimension=1, tiled=True
    ).astype(jnp.float32)
    mixed = (resid_own.astype(jnp.float32) + shared_own + routed).astype(jnp.bfloat16)
    return (mixed, new_real, new_imag)


def solution(mesh):
    placed = (
        P("ep", None),
        P(),
        P(),
        P(None, "tp"),
        P("tp"),
        P("tp"),
        P("tp"),
        P(None, "tp"),
        P(None, "tp"),
        P(None, "tp"),
        P(None, "tp"),
        P("tp"),
        P("ep", "tp"),
        P("ep", "tp"),
        P("tp", None),
        P(None, "tp"),
        P(None, "tp"),
        P("tp", None),
        P("ep", "tp", None),
        P("ep", "tp", None),
        P("ep", None, "tp"),
        P("ep", None),
        P("ep", None),
    )
    return jax.shard_map(
        local,
        mesh=mesh,
        in_specs=placed,
        out_specs=(P("ep", "tp"), P("ep", "tp"), P("ep", "tp")),
        check_vma=False,
    )
```

profile of v0, /device:TPU:0, one launch (start us, length us, event | category | flops | bytes accessed | tf_op | source)
XLA Modules:
  0.0 197.0 jit_solution(18267901409263895610)
XLA Ops:
  7.2 0.0 copy-start
  7.2 0.0 copy-start.7
  7.2 0.0 reduce-scatter.3.cloned.1.call-start
  7.3 0.8 exp.27
  8.1 1.2 fusion.34
  9.4 0.8 reshape.245
  10.1 0.8 mul.328
  10.9 0.7 fusion.74
  11.6 0.1 neg.30
  11.6 0.1 mul.307
  11.7 2.3 %convolution_convert_fusion.2 = bf16[64,256]{1,0:T(8,128)(2,1)S(1)} fusion(bf16[4096,256]{1,0:T(8,128)(2,1)} %param.26, bf16[64,4096]{1,0:T(8,128)(2,1)} %param.23, f32[4096]{0:T(1024)} %param.24, f32[64]{0:T(128)S(1)} %add_rsqrt_fusion), kind=kOutput, calls=%fused_computation.28 | convolution fusion | flops 135282688 | bytes 2670848 | tf_op jit(solution)/shard_map/dot_general | solution.py:35
  14.0 0.1 copy.78
  14.2 0.1 reshape.249
  14.3 0.1 reshape.250
  14.4 0.7 reshape.251
  15.1 0.1 reshape.252
  15.2 1.0 reshape.246
  16.1 0.9 reshape.247
  17.1 0.4 fusion.57
  17.5 0.1 cosine_multiply_fusion
  17.6 1.9 bitcast_add_fusion
  19.6 0.9 fusion.55
  20.5 1.0 fusion.50
  21.5 0.0 copy-start.11
  21.5 1.5 fusion.75
  23.0 0.0 reduce-scatter.3.cloned.1.call-update
  23.1 0.0 all-reduce.3.cloned.1.call-start
  23.1 0.1 copy.85
  23.2 0.1 eq.56
  23.3 0.1 eq.52
  23.5 0.6 reduce-window.6
  24.1 0.2 slice_reduce_fusion
  24.3 0.1 fusion.69
  24.4 0.1 reduce_sum.59
  24.5 0.1 copy.88
  24.6 0.8 dynamic_slice.7
  25.3 0.1 convert_reduce_fusion
  25.5 33.1 %reduce-scatter.3.cloned.1.call-done = f32[64,512]{1,0:T(8,128)} async-done(((f32[64,4096]{1,0:T(8,128)}), f32[64,512]{1,0:T(8,128)}) %reduce-scatter.3.cloned.1.call-update) | async-done | bytes 131088 | tf_op jit(solution)/shard_map/reduce_scatter | solution.py:116
  58.5 1.0 fusion.51
  59.6 13.9 %psum.21 = f32[64,1]{0,1:T(1,128)S(1)} all-reduce(f32[64,1]{0,1:T(1,128)S(1)} %bitcast.105), channel_id=1, replica_groups=mesh['ep'=4,'tp'=8] {'tp'}, use_global_device_ids=true, to_apply=%region_3.0 | all-reduce | flops 64 | bytes 512 | tf_op jit(solution)/shard_map/psum | solution.py:120
  73.4 0.1 fusion.53
  73.5 0.3 convolution_convert_fusion.1
  73.9 11.7 %all_to_all.10 = bf16[4,128,512]{2,1,0:T(8,128)(2,1)S(1)} all-to-all(bf16[4,128,512]{2,1,0:T(8,128)(2,1)S(1)} %bitcast.99), channel_id=1, replica_groups=mesh['ep'=4,'tp'=8] {'ep'}, dimensions={0} | all-to-all | bytes 1048576 | tf_op jit(solution)/shard_map/all_to_all | solution.py:144
  85.6 4.0 %fusion.17 = bf16[4,4,32,1024]{3,2,0,1:T(8,128)(2,1)} fusion(bf16[4,512,1024]{2,1,0:T(8,128)(2,1)} %param.42, bf16[4,4,32,512]{3,2,1,0:T(8,128)(2,1)S(1)} %bitcast.97), kind=kOutput, calls=%fused_computation.16 | convolution fusion | flops 537395200 | bytes 5767168 | tf_op jit(solution)/shard_map/secd,edf->secf/dot_general | solution.py:149
  89.6 1.7 fusion.20
  91.3 0.0 all-reduce.3.cloned.1.call-update
  91.4 0.0 reduce-scatter.5.cloned.1.call-start
  91.4 16.5 %all_gather.3 = bf16[64,4096]{1,0:T(8,128)(2,1)S(1)} all-gather(bf16[64,512]{1,0:T(8,128)(2,1)S(1)} %fusion.53), channel_id=1, replica_groups=mesh['ep'=4,'tp'=8] {'tp'}, dimensions={1}, use_global_device_ids=true | all-gather | bytes 589824 | tf_op jit(solution)/shard_map/all_gather | solution.py:124
  107.9 1.5 fusion.76
  109.5 3.0 %convolution_convert_fusion = bf16[64,4096]{1,0:T(8,128)(2,1)} fusion(bf16[128,4096]{1,0:T(8,128)(2,1)} %param.40, bf16[64,4096]{1,0:T(8,128)(2,1)S(1)} %all_gather.3, bf16[4096,128]{1,0:T(8,128)(2,1)} %param.39, f32[64,128]{1,0:T(8,128)S(1)} %fusion.76), kind=kOutput, calls=%fused_computation | convolution fusion | flops 134529024 | bytes 3178496 | tf_op jit(solution)/shard_map/dot_general | solution.py:172
  112.4 0.0 reduce-scatter.5.cloned.1.call-update
  112.5 42.7 %all-reduce.3.cloned.1.call-done = (bf16[4,4,32,1024]{3,2,0,1:T(8,128)(2,1)}, bf16[4,4,32,1024]{3,2,0,1:T(8,128)(2,1)}) async-done(((bf16[4,4,32,1024]{3,2,0,1:T(8,128)(2,1)}, bf16[4,4,32,1024]{3,2,0,1:T(8,128)(2,1)}), (bf16[4,4,32,1024]{3,2,0,1:T(8,128)(2,1)}, bf16[4,4,32,1024]{3,2,0,1:T(8,128)(2,1)})) %all-reduce.3.cloned.1.call-update) | async-done | bytes 2097168 | tf_op jit(solution)/shard_map/psum | solution.py:152
  155.1 3.7 %fusion.26 = bf16[4,4,32,512]{3,2,0,1:T(8,128)(2,1)S(1)} fusion(bf16[4,1024,512]{2,1,0:T(8,128)(2,1)} %param.43, bf16[4,4,32,1024]{3,2,0,1:T(8,128)(2,1)} %get-tuple-element.3, bf16[4,4,32,1024]{3,2,0,1:T(8,128)(2,1)} %get-tuple-element.4), kind=kOutput, calls=%fused_computation.22 | convolution fusion | flops 541327360 | bytes 6815744 | tf_op jit(solution)/shard_map/secf,efd->secd/dot_general | solution.py:155
  158.9 0.9 copy.91
  159.7 4.1 %all-to-all-start.1 = ((bf16[4,128,512]{2,1,0:T(8,128)(2,1)}), bf16[4,128,512]{2,1,0:T(8,128)(2,1)}, u32[]{:S(2)}, u32[]{:S(2)}) async-start(bf16[4,128,512]{2,1,0:T(8,128)(2,1)} %bitcast.100), calls=%async_computation.3 | async-start | bytes 1048576 | tf_op jit(solution)/shard_map/all_to_all | solution.py:158
  163.9 0.0 copy-start.12
  163.9 1.1 copy.93
  165.0 0.3 copy.92
  165.3 1.9 reshape.259
  167.2 0.9 reshape.258
  168.1 0.1 select_reduce_fusion
  168.3 20.2 %reduce-scatter.5.cloned.1.call-done = bf16[64,512]{1,0:T(8,128)(2,1)} async-done(((bf16[64,4096]{1,0:T(8,128)(2,1)}), bf16[64,512]{1,0:T(8,128)(2,1)}) %reduce-scatter.5.cloned.1.call-update) | async-done | bytes 65552 | tf_op jit(solution)/shard_map/reduce_scatter | solution.py:173
  188.4 0.0 all-to-all-done.1
  188.4 2.1 %fusion.31 = bf16[64,512]{1,0:T(8,128)(2,1)} fusion(f32[64,512]{1,0:T(8,128)S(1)} %select_reduce_fusion, bf16[512,512]{1,0:T(8,128)(2,1)} %bitcast.22, bf16[64,512]{1,0:T(8,128)(2,1)S(1)} %get-tuple-element.6, bf16[64,512]{1,0:T(8,128)(2,1)} %reduce-scatter.5.cloned.1.call-done), kind=kOutput, calls=%fused_computation.27 | convolution fusion | flops 201490432 | bytes 851968 | tf_op jit(solution)/shard_map/dot_general | solution.py:168
  (30 shorter events, 0.1 us)
Async XLA Ops:
  7.2 14.4 %copy-start = (bf16[256,4096]{1,0:T(8,128)(2,1)S(1)}, bf16[256,4096]{1,0:T(8,128)(2,1)}, u32[]{:S(2)}) copy-start(bf16[256,4096]{1,0:T(8,128)(2,1)} %param.37) | copy-start | bytes 6291460
  7.2 7.0 %copy-start.7 = (f32[16,1024]{1,0:T(8,128)S(1)}, f32[16,1024]{1,0:T(8,128)}, u32[]{:S(2)}) copy-start(f32[16,1024]{1,0:T(8,128)} %param.30) | copy-start | bytes 196612
  7.2 7.1 %copy-start.8 = (f32[16,1024]{1,0:T(8,128)S(1)}, f32[16,1024]{1,0:T(8,128)}, u32[]{:S(2)}) copy-start(f32[16,1024]{1,0:T(8,128)} %param.31) | copy-start | bytes 196612
  7.2 7.2 %copy-start.9 = (f32[16,1024]{1,0:T(8,128)S(1)}, f32[16,1024]{1,0:T(8,128)}, u32[]{:S(2)}) copy-start(f32[16,1024]{1,0:T(8,128)} %param.32) | copy-start | bytes 196612
  7.2 7.9 %copy-start.10 = (f32[16,1024]{1,0:T(8,128)S(1)}, f32[16,1024]{1,0:T(8,128)}, u32[]{:S(2)}) copy-start(f32[16,1024]{1,0:T(8,128)} %param.33) | copy-start | bytes 196612
  7.2 8.0 %copy-start.5 = (f32[64,1024]{1,0:T(8,128)S(1)}, f32[64,1024]{1,0:T(8,128)}, u32[]{:S(2)}) copy-start(f32[64,1024]{1,0:T(8,128)} %param.35) | copy-start | bytes 786436
  7.2 51.3 %reduce-scatter.3.cloned.1.call-start = ((), (), s32[]{:S(2)}) async-start(), calls=%async_computation.4 | async-start | bytes 1179648 | tf_op jit(solution)/shard_map/reduce_scatter | solution.py:116
  11.7 4.4 %copy-start.6 = (f32[64,1024]{1,0:T(8,128)S(1)}, f32[64,1024]{1,0:T(8,128)}, u32[]{:S(2)}) copy-start(f32[64,1024]{1,0:T(8,128)} %param.36) | copy-start | bytes 786436
  17.1 2.5 %copy-start.4 = (f32[16,16,64]{2,1,0:T(8,128)S(1)}, f32[16,16,64]{2,1,0:T(8,128)}, u32[]{:S(2)}) copy-start(f32[16,16,64]{2,1,0:T(8,128)} %reshape.251) | copy-start | bytes 196612
  19.6 3.5 %copy-start.1 = (f32[64,16,64]{2,0,1:T(8,128)}, f32[64,16,64]{2,0,1:T(8,128)S(1)}, u32[]{:S(2)}) copy-start(f32[64,16,64]{2,0,1:T(8,128)S(1)} %get-tuple-element.7) | copy-start | bytes 786436
  21.5 1.6 copy-start.11
  23.1 132.1 %all-reduce.3.cloned.1.call-start = ((), (), s32[]{:S(2)}) async-start(), calls=%async_computation.6 | async-start | bytes 4194304 | tf_op jit(solution)/shard_map/psum | solution.py:152
  85.6 4.0 %copy-start.3 = (bf16[4,512,1024]{2,1,0:T(8,128)(2,1)S(1)}, bf16[4,512,1024]{2,1,0:T(8,128)(2,1)}, u32[]{:S(2)}) copy-start(bf16[4,512,1024]{2,1,0:T(8,128)(2,1)} %param.41) | copy-start | bytes 12582916
  91.4 97.0 %reduce-scatter.5.cloned.1.call-start = ((), (), s32[]{:S(2)}) async-start(), calls=%async_computation.5 | async-start | bytes 589824 | tf_op jit(solution)/shard_map/reduce_scatter | solution.py:173
  158.8 5.0 %copy-start.2 = (f32[64,16,64]{2,0,1:T(8,128)S(1)}, f32[64,16,64]{2,0,1:T(8,128)}, u32[]{:S(2)}) copy-start(f32[64,16,64]{2,0,1:T(8,128)} %copy-done.1) | copy-start | bytes 786436
  159.7 28.7 %all-to-all-start.1 = ((bf16[4,128,512]{2,1,0:T(8,128)(2,1)}), bf16[4,128,512]{2,1,0:T(8,128)(2,1)}, u32[]{:S(2)}, u32[]{:S(2)}) async-start(bf16[4,128,512]{2,1,0:T(8,128)(2,1)} %bitcast.100), calls=%async_computation.3 | async-start | bytes 1048576 | tf_op jit(solution)/shard_map/all_to_all | solution.py:158
  163.9 4.2 %copy-start.12 = (f32[64,4]{0,1:T(4,128)S(1)}, f32[64,4]{0,1:T(4,128)}, u32[]{:S(2)}) copy-start(f32[64,4]{0,1:T(4,128)} %param.45) | copy-start | bytes 3076
Sparse Core Ops, SparseCore 0:
  23.2 35.2 reduce-scatter.2
  91.5 63.6 all-reduce.2
  157.4 30.9 reduce-scatter.4
where the time goes:
time: 198 us; the launch traced here: 197 us
  waiting for transfers between devices  96 us (48%)
  blocking collectives  42.1 us (21%)
  matrix products  24.4 us (12%)
  between operations  14 us (7%)
  local copies, waits for them, and re-layouts  12 us (6%)
  starting transfers between devices  4.25 us (2%)
  other arithmetic  4.21 us (2%)
    psum x1, waiting for transfers between devices, local(): lax.psum(up_part.astype(jnp.bfloat16), 'tp').astype(jnp.float32)  42.7 us
    reduce_scatter x1, waiting for transfers between devices, local(): lax.psum_scatter(mixer_terms, 'tp', scatter_dimension=1, tiled=True)  33.1 us
    reduce_scatter x1, waiting for transfers between devices, local(): lax.psum_scatter(shared_terms.astype(jnp.bfloat16), 'tp', scatter_dimensi...  20.2 us
    all_gather x1, blocking collectives, local(): ffn_rows = lax.all_gather(rows_own, 'tp', axis=1, tiled=True)  16.5 us
    psum x1, blocking collectives, local(): lax.psum(jnp.sum(resid_f * resid_f, axis=1, keepdims=True), 'tp')  13.9 us
    all_to_all x1, blocking collectives, local(): lax.all_to_all(outgoing, 'ep', split_axis=0, concat_axis=0, tiled=True)  11.7 us
    all_to_all x1, starting transfers between devices, local(): lax.all_to_all(expert_terms.reshape(ep_count, expert_dev * capacity, slic...  4.13 us
    dot_general x1, matrix products, local(): jnp.einsum('secd,edf->secf', arrived, expert_up, preferred_element_type=j...  4.04 us
  transfers between devices with their start and end apart: 4, of which 3 were waited for; matrix products, arithmetic and copies ran while one was open for 8% of the time, Pallas kernels for 0%

commit v1 on v0

--- a/solution.py
+++ b/solution.py
@@ -121,7 +121,9 @@
     factor = lax.rsqrt(square_sum / model_width + EPS)
     gain_own = lax.dynamic_slice_in_dim(ffn_gain, offset, slice_width, 0)
     rows_own = (resid_f * factor * gain_own).astype(jnp.bfloat16)
-    ffn_rows = lax.all_gather(rows_own, "tp", axis=1, tiled=True)
+    ffn_rows = jnp.concatenate(
+        lax.all_to_all(jnp.stack([rows_own] * lax.axis_size("tp")), "tp", 0, 0), axis=1
+    )
     expert_dev = expert_gate.shape[0]
     expert_count = expert_dev * ep_count
     top_count = routing.shape[1]

time: 198 us -> 204 us (1.030)
  waiting for transfers between devices: 96 us -> 113 us
  blocking collectives: 42.1 us -> 25.6 us
  starting transfers between devices: 4.25 us -> 8.39 us
    all_gather x1 -> x0, blocking collectives: 16.5 us -> none  [local(): ffn_rows = lax.all_gather(rows_own, 'tp', axis=1, tiled=True)]
    all_to_all x0 -> x1, waiting for transfers between devices: none -> 11.1 us  [local(): lax.all_to_all(jnp.stack([rows_own] * lax.axis_size('tp')), 'tp', 0, 0)]
    psum x1, waiting for transfers between devices: 42.7 us -> 48.3 us  [local(): lax.psum(up_part.astype(jnp.bfloat16), 'tp').astype(jnp.float32)]
    all_to_all x0 -> x1, starting transfers between devices: none -> 4.14 us  [local(): lax.all_to_all(jnp.stack([rows_own] * lax.axis_size('tp')), 'tp', 0, 0)]
    reduce_scatter x1, waiting for transfers between devices: 20.2 us -> 17.5 us  [local(): lax.psum_scatter(shared_terms.astype(jnp.bfloat16), 'tp', scatter_dimensi...]
    all_to_all x1, waiting for transfers between devices: 0.01 us -> 2.63 us  [local(): lax.all_to_all(expert_terms.reshape(ep_count, expert_dev * capacity, slic...]
  transfers between devices with their start and end apart: 4 -> 5, of which waited for: 3 -> 5; matrix products, arithmetic and copies ran while one was open for 8% -> 11% of each run, Pallas kernels for 0% -> 0%
where the time goes in v1:
time: 204 us; the launch traced here: 203 us
  waiting for transfers between devices  113 us (55%)
  blocking collectives  25.6 us (13%)
  matrix products  24.4 us (12%)
  local copies, waits for them, and re-layouts  14 us (7%)
  between operations  14 us (7%)
  starting transfers between devices  8.39 us (4%)
  other arithmetic  4.21 us (2%)
    psum x1, waiting for transfers between devices, local(): lax.psum(up_part.astype(jnp.bfloat16), 'tp').astype(jnp.float32)  48.3 us
    reduce_scatter x1, waiting for transfers between devices, local(): lax.psum_scatter(mixer_terms, 'tp', scatter_dimension=1, tiled=True)  33.1 us
    reduce_scatter x1, waiting for transfers between devices, local(): lax.psum_scatter(shared_terms.astype(jnp.bfloat16), 'tp', scatter_dimensi...  17.5 us
    psum x1, blocking collectives, local(): lax.psum(jnp.sum(resid_f * resid_f, axis=1, keepdims=True), 'tp')  13.9 us
    all_to_all x1, blocking collectives, local(): lax.all_to_all(outgoing, 'ep', split_axis=0, concat_axis=0, tiled=True)  11.7 us
    all_to_all x1, waiting for transfers between devices, local(): lax.all_to_all(jnp.stack([rows_own] * lax.axis_size('tp')), 'tp', 0, 0)  11.1 us
    all_to_all x1, starting transfers between devices, local(): lax.all_to_all(jnp.stack([rows_own] * lax.axis_size('tp')), 'tp', 0, 0)  4.14 us
    all_to_all x1, starting transfers between devices, local(): lax.all_to_all(expert_terms.reshape(ep_count, expert_dev * capacity, slic...  4.13 us
  transfers between devices with their start and end apart: 5, of which 5 were waited for; matrix products, arithmetic and copies ran while one was open for 11% of the time, Pallas kernels for 0%

profile of v1, /device:TPU:0, one launch (start us, length us, event | category | flops | bytes accessed | tf_op | source)
XLA Modules:
  0.0 203.4 jit_solution(6306441812614576240)
XLA Ops:
  7.2 0.0 copy-start
  7.2 0.0 reduce-scatter.3.cloned.1.call-start
  7.3 0.8 exp.27
  8.1 1.2 fusion.34
  9.4 0.8 reshape.253
  10.1 0.8 mul.328
  10.9 0.7 fusion.74
  11.6 0.1 neg.30
  11.6 0.1 mul.307
  11.7 2.3 %convolution_convert_fusion.2 = bf16[64,256]{1,0:T(8,128)(2,1)S(1)} fusion(bf16[4096,256]{1,0:T(8,128)(2,1)} %param.26, bf16[64,4096]{1,0:T(8,128)(2,1)} %param.23, f32[4096]{0:T(1024)} %param.24, f32[64]{0:T(128)S(1)} %add_rsqrt_fusion), kind=kOutput, calls=%fused_computation.28 | convolution fusion | flops 135282688 | bytes 2670848 | tf_op jit(solution)/shard_map/dot_general | solution.py:35
  14.0 0.1 copy.100
  14.2 0.1 reshape.257
  14.3 0.1 reshape.258
  14.4 0.7 reshape.259
  15.1 0.1 reshape.260
  15.2 1.0 reshape.254
  16.1 0.9 reshape.255
  17.1 0.4 fusion.57
  17.5 0.1 cosine_multiply_fusion
  17.6 1.9 bitcast_add_fusion
  19.6 0.9 fusion.55
  20.5 1.0 fusion.50
  21.5 1.5 fusion.75
  23.0 0.0 reduce-scatter.3.cloned.1.call-update
  23.1 0.1 copy.108
  23.2 0.1 eq.56
  23.3 0.1 eq.52
  23.4 0.6 reduce-window.6
  24.0 0.2 slice_reduce_fusion
  24.2 0.1 fusion.69
  24.3 0.1 reduce_sum.59
  24.4 0.1 copy.111
  24.5 0.8 dynamic_slice.7
  25.3 0.1 convert_reduce_fusion
  25.4 33.1 %reduce-scatter.3.cloned.1.call-done = f32[64,512]{1,0:T(8,128)} async-done(((f32[64,4096]{1,0:T(8,128)}), f32[64,512]{1,0:T(8,128)}) %reduce-scatter.3.cloned.1.call-update) | async-done | bytes 131088 | tf_op jit(solution)/shard_map/reduce_scatter | solution.py:116
  58.5 1.0 fusion.51
  59.6 13.9 %psum.21 = f32[64,1]{0,1:T(1,128)S(1)} all-reduce(f32[64,1]{0,1:T(1,128)S(1)} %bitcast.110), channel_id=1, replica_groups=mesh['ep'=4,'tp'=8] {'tp'}, use_global_device_ids=true, to_apply=%region_3.0 | all-reduce | flops 64 | bytes 512 | tf_op jit(solution)/shard_map/psum | solution.py:120
  73.4 0.1 fusion.53
  73.5 0.3 convolution_convert_fusion.1
  73.9 11.7 %all_to_all.15 = bf16[4,128,512]{2,1,0:T(8,128)(2,1)S(1)} all-to-all(bf16[4,128,512]{2,1,0:T(8,128)(2,1)S(1)} %bitcast.104), channel_id=1, replica_groups=mesh['ep'=4,'tp'=8] {'ep'}, dimensions={0} | all-to-all | bytes 1048576 | tf_op jit(solution)/shard_map/all_to_all | solution.py:146
  85.6 0.8 stack.2
  86.4 4.1 %all-to-all-start = ((bf16[8,64,512]{2,1,0:T(8,128)(2,1)}), bf16[8,64,512]{2,1,0:T(8,128)(2,1)}, u32[]{:S(2)}, u32[]{:S(2)}) async-start(bf16[8,64,512]{2,1,0:T(8,128)(2,1)} %stack.2), calls=%async_computation.1 | async-start | bytes 1048576 | tf_op jit(solution)/shard_map/all_to_all | solution.py:125
  90.6 0.0 all-reduce.3.cloned.1.call-start
  90.7 4.0 %fusion.17 = bf16[4,4,32,1024]{3,2,0,1:T(8,128)(2,1)} fusion(bf16[4,512,1024]{2,1,0:T(8,128)(2,1)} %param.42, bf16[4,4,32,512]{3,2,1,0:T(8,128)(2,1)S(1)} %bitcast.102), kind=kOutput, calls=%fused_computation.16 | convolution fusion | flops 537395200 | bytes 5767168 | tf_op jit(solution)/shard_map/secd,edf->secf/dot_general | solution.py:151
  94.7 1.7 fusion.20
  96.4 0.0 all-reduce.3.cloned.1.call-update
  96.4 0.0 reduce-scatter.5.cloned.1.call-start
  96.5 11.1 %all-to-all-done = bf16[8,64,512]{2,1,0:T(8,128)(2,1)} async-done(((bf16[8,64,512]{2,1,0:T(8,128)(2,1)}), bf16[8,64,512]{2,1,0:T(8,128)(2,1)}, u32[]{:S(2)}, u32[]{:S(2)}) %all-to-all-start) | async-done | bytes 524320 | tf_op jit(solution)/shard_map/all_to_all | solution.py:125
  107.6 1.1 copy.120
  108.7 1.6 fusion.76
  110.2 3.0 %convolution_convert_fusion = bf16[64,4096]{1,0:T(8,128)(2,1)} fusion(bf16[128,4096]{1,0:T(8,128)(2,1)} %param.40, bf16[64,4096]{1,0:T(8,128)(2,1)S(1)} %bitcast.101, bf16[4096,128]{1,0:T(8,128)(2,1)} %param.39, f32[64,128]{1,0:T(8,128)S(1)} %fusion.76), kind=kOutput, calls=%fused_computation | convolution fusion | flops 134529024 | bytes 3178496 | tf_op jit(solution)/shard_map/dot_general | solution.py:174
  113.2 0.0 reduce-scatter.5.cloned.1.call-update
  113.2 48.3 %all-reduce.3.cloned.1.call-done = (bf16[4,4,32,1024]{3,2,0,1:T(8,128)(2,1)}, bf16[4,4,32,1024]{3,2,0,1:T(8,128)(2,1)}) async-done(((bf16[4,4,32,1024]{3,2,0,1:T(8,128)(2,1)}, bf16[4,4,32,1024]{3,2,0,1:T(8,128)(2,1)}), (bf16[4,4,32,1024]{3,2,0,1:T(8,128)(2,1)}, bf16[4,4,32,1024]{3,2,0,1:T(8,128)(2,1)})) %all-reduce.3.cloned.1.call-update) | async-done | bytes 2097168 | tf_op jit(solution)/shard_map/psum | solution.py:154
  161.6 3.7 %fusion.26 = bf16[4,4,32,512]{3,2,0,1:T(8,128)(2,1)S(1)} fusion(bf16[4,1024,512]{2,1,0:T(8,128)(2,1)} %param.43, bf16[4,4,32,1024]{3,2,0,1:T(8,128)(2,1)} %get-tuple-element.3, bf16[4,4,32,1024]{3,2,0,1:T(8,128)(2,1)} %get-tuple-element.4), kind=kOutput, calls=%fused_computation.22 | convolution fusion | flops 541327360 | bytes 6815744 | tf_op jit(solution)/shard_map/secf,efd->secd/dot_general | solution.py:157
  165.3 0.9 copy.114
  166.1 4.1 %all-to-all-start.2 = ((bf16[4,128,512]{2,1,0:T(8,128)(2,1)}), bf16[4,128,512]{2,1,0:T(8,128)(2,1)}, u32[]{:S(2)}, u32[]{:S(2)}) async-start(bf16[4,128,512]{2,1,0:T(8,128)(2,1)} %bitcast.105), calls=%async_computation.4 | async-start | bytes 1048576 | tf_op jit(solution)/shard_map/all_to_all | solution.py:160
  170.3 1.1 copy.116
  171.4 0.3 copy.115
  171.7 1.9 reshape.269
  173.6 0.9 reshape.268
  174.5 0.1 select_reduce_fusion
  174.7 2.6 %all-to-all-done.2 = bf16[4,128,512]{2,1,0:T(8,128)(2,1)} async-done(((bf16[4,128,512]{2,1,0:T(8,128)(2,1)}), bf16[4,128,512]{2,1,0:T(8,128)(2,1)}, u32[]{:S(2)}, u32[]{:S(2)}) %all-to-all-start.2) | async-done | bytes 524320 | tf_op jit(solution)/shard_map/all_to_all | solution.py:160
  177.3 17.5 %reduce-scatter.5.cloned.1.call-done = bf16[64,512]{1,0:T(8,128)(2,1)} async-done(((bf16[64,4096]{1,0:T(8,128)(2,1)}), bf16[64,512]{1,0:T(8,128)(2,1)}) %reduce-scatter.5.cloned.1.call-update) | async-done | bytes 65552 | tf_op jit(solution)/shard_map/reduce_scatter | solution.py:175
  194.8 2.1 %fusion.31 = bf16[64,512]{1,0:T(8,128)(2,1)} fusion(f32[64,512]{1,0:T(8,128)S(1)} %select_reduce_fusion, bf16[512,512]{1,0:T(8,128)(2,1)} %bitcast.23, bf16[64,512]{1,0:T(8,128)(2,1)S(1)} %get-tuple-element.6, bf16[64,512]{1,0:T(8,128)(2,1)} %reduce-scatter.5.cloned.1.call-done), kind=kOutput, calls=%fused_computation.27 | convolution fusion | flops 201490432 | bytes 851968 | tf_op jit(solution)/shard_map/dot_general | solution.py:170
  (33 shorter events, 0.2 us)
Async XLA Ops:
  7.2 14.4 %copy-start = (bf16[256,4096]{1,0:T(8,128)(2,1)S(1)}, bf16[256,4096]{1,0:T(8,128)(2,1)}, u32[]{:S(2)}) copy-start(bf16[256,4096]{1,0:T(8,128)(2,1)} %param.37) | copy-start | bytes 6291460
  7.2 7.0 %copy-start.7 = (f32[16,1024]{1,0:T(8,128)S(1)}, f32[16,1024]{1,0:T(8,128)}, u32[]{:S(2)}) copy-start(f32[16,1024]{1,0:T(8,128)} %param.30) | copy-start | bytes 196612
  7.2 7.1 %copy-start.8 = (f32[16,1024]{1,0:T(8,128)S(1)}, f32[16,1024]{1,0:T(8,128)}, u32[]{:S(2)}) copy-start(f32[16,1024]{1,0:T(8,128)} %param.31) | copy-start | bytes 196612
  7.2 7.2 %copy-start.9 = (f32[16,1024]{1,0:T(8,128)S(1)}, f32[16,1024]{1,0:T(8,128)}, u32[]{:S(2)}) copy-start(f32[16,1024]{1,0:T(8,128)} %param.32) | copy-start | bytes 196612
  7.2 7.9 %copy-start.10 = (f32[16,1024]{1,0:T(8,128)S(1)}, f32[16,1024]{1,0:T(8,128)}, u32[]{:S(2)}) copy-start(f32[16,1024]{1,0:T(8,128)} %param.33) | copy-start | bytes 196612
  7.2 8.0 %copy-start.5 = (f32[64,1024]{1,0:T(8,128)S(1)}, f32[64,1024]{1,0:T(8,128)}, u32[]{:S(2)}) copy-start(f32[64,1024]{1,0:T(8,128)} %param.35) | copy-start | bytes 786436
  7.2 51.3 %reduce-scatter.3.cloned.1.call-start = ((), (), s32[]{:S(2)}) async-start(), calls=%async_computation.5 | async-start | bytes 1179648 | tf_op jit(solution)/shard_map/reduce_scatter | solution.py:116
  11.7 4.4 %copy-start.6 = (f32[64,1024]{1,0:T(8,128)S(1)}, f32[64,1024]{1,0:T(8,128)}, u32[]{:S(2)}) copy-start(f32[64,1024]{1,0:T(8,128)} %param.36) | copy-start | bytes 786436
  17.1 2.5 %copy-start.4 = (f32[16,16,64]{2,1,0:T(8,128)S(1)}, f32[16,16,64]{2,1,0:T(8,128)}, u32[]{:S(2)}) copy-start(f32[16,16,64]{2,1,0:T(8,128)} %reshape.259) | copy-start | bytes 196612
  19.6 3.5 %copy-start.1 = (f32[64,16,64]{2,0,1:T(8,128)}, f32[64,16,64]{2,0,1:T(8,128)S(1)}, u32[]{:S(2)}) copy-start(f32[64,16,64]{2,0,1:T(8,128)S(1)} %get-tuple-element.7) | copy-start | bytes 786436
  21.5 1.5 copy-start.11
  86.4 21.2 %all-to-all-start = ((bf16[8,64,512]{2,1,0:T(8,128)(2,1)}), bf16[8,64,512]{2,1,0:T(8,128)(2,1)}, u32[]{:S(2)}, u32[]{:S(2)}) async-start(bf16[8,64,512]{2,1,0:T(8,128)(2,1)} %stack.2), calls=%async_computation.1 | async-start | bytes 1048576 | tf_op jit(solution)/shard_map/all_to_all | solution.py:125
  90.6 71.0 %all-reduce.3.cloned.1.call-start = ((), (), s32[]{:S(2)}) async-start(), calls=%async_computation.7 | async-start | bytes 4194304 | tf_op jit(solution)/shard_map/psum | solution.py:154
  90.6 4.1 %copy-start.3 = (bf16[4,512,1024]{2,1,0:T(8,128)(2,1)S(1)}, bf16[4,512,1024]{2,1,0:T(8,128)(2,1)}, u32[]{:S(2)}) copy-start(bf16[4,512,1024]{2,1,0:T(8,128)(2,1)} %param.41) | copy-start | bytes 12582916
  96.4 98.4 %reduce-scatter.5.cloned.1.call-start = ((), (), s32[]{:S(2)}) async-start(), calls=%async_computation.6 | async-start | bytes 589824 | tf_op jit(solution)/shard_map/reduce_scatter | solution.py:175
  165.3 5.0 %copy-start.2 = (f32[64,16,64]{2,0,1:T(8,128)S(1)}, f32[64,16,64]{2,0,1:T(8,128)}, u32[]{:S(2)}) copy-start(f32[64,16,64]{2,0,1:T(8,128)} %copy-done.1) | copy-start | bytes 786436
  166.1 11.2 %all-to-all-start.2 = ((bf16[4,128,512]{2,1,0:T(8,128)(2,1)}), bf16[4,128,512]{2,1,0:T(8,128)(2,1)}, u32[]{:S(2)}, u32[]{:S(2)}) async-start(bf16[4,128,512]{2,1,0:T(8,128)(2,1)} %bitcast.105), calls=%async_computation.4 | async-start | bytes 1048576 | tf_op jit(solution)/shard_map/all_to_all | solution.py:160
  170.3 4.2 %copy-start.12 = (f32[64,4]{0,1:T(4,128)S(1)}, f32[64,4]{0,1:T(4,128)}, u32[]{:S(2)}) copy-start(f32[64,4]{0,1:T(4,128)} %param.45) | copy-start | bytes 3076
Sparse Core Ops, SparseCore 0:
  23.2 35.2 reduce-scatter.2
  96.5 64.9 all-reduce.2
  163.8 30.9 reduce-scatter.4
